TPU v7x, 32 devices: a whole 2x2x4 slice. The times are simulated.
32 devices in a mesh: grp: 2 (over y), sp: 8 (over z, core), tp: 2 (over x).
Axes of the slice: x: 2, y: 2, z: 4, core: 2. Of those that a mesh axis runs over, the one named last changes fastest.
Arguments:
- queries_a: bfloat16 [4096, 2, 512], P(('grp', 'sp'), None, 'tp'), parts along dimension 0, may hold values from -120 to 120
- keys_a: bfloat16 [4096, 2, 512], P(('grp', 'sp'), None, 'tp'), parts along dimension 0, may hold values from -6 to 6
- values_a: bfloat16 [4096, 1024], P(('grp', 'sp'), 'tp'), parts along dimension 0, may hold values from -6 to 6
- queries_b: bfloat16 [4096, 2, 512], P(('grp', 'sp'), None, 'tp'), parts along dimension 0, may hold values from -120 to 120
- keys_b: bfloat16 [4096, 2, 512], P(('grp', 'sp'), None, 'tp'), parts along dimension 0, may hold values from -6 to 6
- values_b: bfloat16 [4096, 1024], P(('grp', 'sp'), 'tp'), parts along dimension 0, may hold values from -6 to 6
- lambdas: float32 [12], replicated, may hold values from 0.3 to 0.8
- head_gain_a: float32 [256], replicated, may hold values from 0.1 to 1.9
- head_gain_b: float32 [128], replicated, may hold values from 0.1 to 1.9
- out_a: bfloat16 [1024, 2048], P('tp'), may hold values from -0.125 to 0.125
- out_b: bfloat16 [1024, 2048], P('tp'), may hold values from -0.125 to 0.125
- residual: bfloat16 [4096, 2048], P(('grp', 'sp', 'tp')), parts along dimension 0, may hold values from -6 to 6
- gain_mix: float32 [2048], replicated, may hold values from 0.1 to 1.9
- gain_pre: float32 [2048], replicated, may hold values from 0.1 to 1.9
- gain_post: float32 [2048], replicated, may hold values from 0.1 to 1.9
- routes: int32 [4096, 4], P(('grp', 'sp', 'tp')), parts along dimension 0, may hold values from 0 to 7, all different within a row; in each aligned block of 128 rows (0 to 127, 128 to 255, ...) at most 80 rows name the same one
- route_weights: float32 [4096, 4], P(('grp', 'sp', 'tp')), parts along dimension 0, may hold values from 0.05 to 1
- expert_gate: bfloat16 [8, 2048, 2048], P('sp', None, 'tp'), may hold values from -1 to 1
- expert_up: bfloat16 [8, 2048, 2048], P('sp', None, 'tp'), may hold values from -1 to 1
- expert_down: bfloat16 [8, 2048, 2048], P('sp', 'tp'), may hold values from -0.125 to 0.125
Outputs:
- layer_out: bfloat16 [4096, 2048], P(('grp', 'sp', 'tp')), parts along dimension 0
There are 2 independent parts, one for each index of `grp`. A program takes and returns all parts, laid end to end along the dimension named above; an argument that names none is the same for every part. Nothing has to cross between parts.
Inputs may be any that keep to these rules, and one draw needn't show every extreme that they name: `routes`: in each aligned block of 128 rows (the rows of one device) no expert is named by more than 80 rows, a bound that some blocks reach.
All inputs are finite; a program needn't handle non-finite values.
Results may differ from a plain program's by a relative error of at most 0.018.
Values may be sent and summed in bfloat16 or wider, within the bound.
A program may use at most 128 MiB of HBM per device.

v0:
```python
import jax
import jax.numpy as jnp
from jax import lax
from jax.sharding import PartitionSpec as P

HA = 4
DA = 128
DB = 64


def rms_norm(values, gain_vec):
    return values * lax.rsqrt(jnp.mean(values * values, -1, keepdims=True) + 1e-06) * gain_vec


def attend(current, query_rows, key_rows, value_rows, first_row, query_pos, head_size):
    run_max, run_sum, run_acc = current
    key_count = key_rows.shape[0]
    heads = query_rows.shape[2]
    key_view = key_rows.reshape(key_count, 2, heads, head_size)
    value_view = value_rows.reshape(key_count, heads, 2 * head_size)
    key_pos = first_row + jnp.arange(key_count, dtype=jnp.int32)
    visible = (key_pos[None, :] <= query_pos[:, None])[None, :, None, :]
    scores = jnp.einsum(
        "qmhd,kmhd->mqhk", query_rows, key_view, preferred_element_type=jnp.float32
    ) * head_size ** (-0.5)
    scores = jnp.where(visible, scores, -1e30)
    new_max = jnp.maximum(run_max, jnp.max(scores, -1))
    exp_terms = jnp.where(visible, jnp.exp(scores - new_max[..., None]), 0.0)
    rescale = jnp.exp(run_max - new_max)
    run_sum = run_sum * rescale + jnp.sum(exp_terms, -1)
    run_acc = run_acc * rescale[..., None] + jnp.einsum(
        "mqhk,khe->mqhe",
        exp_terms.astype(jnp.bfloat16),
        value_view,
        preferred_element_type=jnp.float32,
    )
    return (new_max, run_sum, run_acc)


def fresh_state(length, heads, head_size):
    return (
        jnp.full((2, length, heads), -1e30, jnp.float32),
        jnp.zeros((2, length, heads), jnp.float32),
        jnp.zeros((2, length, heads, 2 * head_size), jnp.float32),
    )


def finish(current, weights_two, gain_vec):
    run_max, run_sum, run_acc = current
    mixture = (
        run_acc[0] / run_sum[0][..., None]
        - weights_two[None, :, None] * run_acc[1] / run_sum[1][..., None]
    )
    normed = rms_norm(mixture, gain_vec)
    return normed.reshape(normed.shape[0], -1).astype(jnp.bfloat16)


def slot_numbers(flat_ids, experts):
    onehot = (flat_ids[:, None] == jnp.arange(experts, dtype=jnp.int32)[None, :]).astype(jnp.int32)
    before = jnp.cumsum(onehot, 0) - onehot
    return jnp.sum(before * onehot, 1)


def send_matrix(route_rows, experts, capacity):
    groups, sub_rows, top_count = route_rows.shape
    slot_ids = jax.vmap(lambda flat_ids: slot_numbers(flat_ids, experts))(
        route_rows.reshape(groups, -1)
    )
    group_ids = jnp.arange(groups, dtype=jnp.int32)[:, None]
    row_ids = (
        route_rows.reshape(groups, -1) * (groups * capacity) + group_ids * capacity + slot_ids
    ).reshape(-1)
    col_ids = jnp.broadcast_to(
        group_ids[:, :, None] * sub_rows + jnp.arange(sub_rows, dtype=jnp.int32)[None, :, None],
        route_rows.shape,
    ).reshape(-1)
    row_hot = (
        row_ids[:, None] == jnp.arange(experts * groups * capacity, dtype=jnp.int32)[None, :]
    ).astype(jnp.bfloat16)
    col_hot = (col_ids[:, None] == jnp.arange(groups * sub_rows, dtype=jnp.int32)[None, :]).astype(
        jnp.bfloat16
    )
    return jnp.einsum("ar,ac->rc", row_hot, col_hot, preferred_element_type=jnp.float32).astype(
        jnp.bfloat16
    )


def back_matrix(route_rows, route_weights, experts, capacity):
    sub_rows, top_count = route_rows.shape
    slot_ids = slot_numbers(route_rows.reshape(-1), experts)
    row_ids = route_rows.reshape(-1) * capacity + slot_ids
    col_ids = jnp.repeat(jnp.arange(sub_rows, dtype=jnp.int32), top_count)
    row_hot = (row_ids[:, None] == jnp.arange(experts * capacity, dtype=jnp.int32)[None, :]).astype(
        jnp.float32
    )
    tok_weighted = (col_ids[:, None] == jnp.arange(sub_rows, dtype=jnp.int32)[None, :]).astype(
        jnp.float32
    ) * route_weights.reshape(-1)[:, None]
    return jnp.einsum("at,ar->tr", tok_weighted, row_hot, precision=lax.Precision.HIGHEST)


def per_device(
    queries_a,
    keys_a,
    values_a,
    queries_b,
    keys_b,
    values_b,
    lambdas,
    head_gain_a,
    head_gain_b,
    out_a,
    out_b,
    residual,
    gain_mix,
    gain_pre,
    gain_post,
    routes,
    route_weights,
    expert_gate,
    expert_up,
    expert_down,
):
    length = queries_a.shape[0]
    heads_a = queries_a.shape[2] // DA
    heads_b = queries_b.shape[2] // DB
    head_slot = lax.axis_index("tp")
    seq_slot = lax.axis_index("sp")
    lambda_a = lax.dynamic_slice_in_dim(lambdas, head_slot * heads_a, heads_a)
    lambda_b = lax.dynamic_slice_in_dim(lambdas, HA + head_slot * heads_b, heads_b)
    groups = [
        (
            queries_a.reshape(length, 2, heads_a, DA),
            queries_b.reshape(length, 2, heads_b, DB),
            seq_slot * length + jnp.arange(length, dtype=jnp.int32),
            seq_slot * length + length - 1,
        )
    ]
    initial = tuple(
        (
            (
                fresh_state(group[2].shape[0], heads_a, DA),
                fresh_state(group[2].shape[0], heads_b, DB),
            )
            for group in groups
        )
    )
    pieces = (
        lax.all_gather(keys_a, "sp", axis=0, tiled=True),
        lax.all_gather(values_a, "sp", axis=0, tiled=True),
        lax.all_gather(keys_b, "sp", axis=0, tiled=True),
        lax.all_gather(values_b, "sp", axis=0, tiled=True),
    )
    key_count = pieces[0].shape[0]
    span_rows = 1024

    def one_span(span_index, carried):
        offset = span_index * span_rows
        parts = tuple(
            (lax.dynamic_slice_in_dim(piece_part, offset, span_rows, 0) for piece_part in pieces)
        )
        group_qa, group_qb, group_pos, group_last = groups[0]

        def compute(inner, group_qa=group_qa, group_qb=group_qb, group_pos=group_pos):
            return (
                attend(inner[0], group_qa, parts[0], parts[1], offset, group_pos, DA),
                attend(inner[1], group_qb, parts[2], parts[3], offset, group_pos, DB),
            )

        updated = [lax.cond(offset <= group_last, compute, lambda inner: inner, carried[0])]
        return tuple(updated)

    final_state = lax.fori_loop(0, key_count // span_rows, one_span, initial)
    heads_out_a = finish(final_state[0][0], lambda_a, head_gain_a)
    heads_out_b = finish(final_state[0][1], lambda_b, head_gain_b)
    mixed_rows = lax.psum_scatter(
        (
            jnp.dot(heads_out_a, out_a, preferred_element_type=jnp.float32)
            + jnp.dot(heads_out_b, out_b, preferred_element_type=jnp.float32)
        ).astype(jnp.bfloat16),
        "tp",
        scatter_dimension=0,
        tiled=True,
    ).astype(jnp.float32)
    after_mix = (residual.astype(jnp.float32) + rms_norm(mixed_rows, gain_mix)).astype(jnp.bfloat16)
    normed = rms_norm(after_mix.astype(jnp.float32), gain_pre).astype(jnp.bfloat16)
    experts = lax.axis_size("sp")
    sub_rows = residual.shape[0]
    top_count = routes.shape[1]
    capacity = min(sub_rows, (5 * sub_rows * top_count + 4 * experts - 1) // (4 * experts))
    width = residual.shape[1]
    outgoing = jnp.dot(
        send_matrix(routes[None], experts, capacity), normed, preferred_element_type=jnp.float32
    ).astype(jnp.bfloat16)
    outgoing = outgoing.reshape(experts, capacity, width)
    arrived = lax.all_to_all(outgoing, "sp", split_axis=0, concat_axis=0, tiled=True)
    sources, slot_count, columns = arrived.shape
    piece_rows = lax.all_gather(arrived.reshape(-1, columns), "tp", axis=0, tiled=True)
    gate_pre = jnp.dot(piece_rows, expert_gate[0], preferred_element_type=jnp.float32)
    up_pre = jnp.dot(piece_rows, expert_up[0], preferred_element_type=jnp.float32)
    glu_part = jnp.minimum(gate_pre, 7.0)
    lin_part = jnp.clip(up_pre, -7.0, 7.0)
    hidden = (glu_part * jax.nn.sigmoid(1.702 * glu_part) * (lin_part + 1.0)).astype(jnp.bfloat16)
    partials = jnp.dot(hidden, expert_down[0], preferred_element_type=jnp.float32)
    mine = lax.psum_scatter(partials.astype(jnp.bfloat16), "tp", scatter_dimension=0, tiled=True)
    results = mine.reshape(sources, slot_count, columns)
    returned = lax.all_to_all(results, "sp", split_axis=0, concat_axis=0, tiled=True)
    combine = back_matrix(routes, route_weights, experts, capacity)
    routed = jnp.dot(
        combine,
        returned.reshape(-1, width).astype(jnp.float32),
        precision=lax.Precision.HIGHEST,
        preferred_element_type=jnp.float32,
    )
    return (after_mix.astype(jnp.float32) + rms_norm(routed, gain_post)).astype(jnp.bfloat16)


def solution(mesh):
    in_specs = (
        P(("grp", "sp"), None, "tp"),
        P(("grp", "sp"), None, "tp"),
        P(("grp", "sp"), "tp"),
        P(("grp", "sp"), None, "tp"),
        P(("grp", "sp"), None, "tp"),
        P(("grp", "sp"), "tp"),
        P(),
        P(),
        P(),
        P("tp", None),
        P("tp", None),
        P(("grp", "sp", "tp"), None),
        P(),
        P(),
        P(),
        P(("grp", "sp", "tp"), None),
        P(("grp", "sp", "tp"), None),
        P("sp", None, "tp"),
        P("sp", None, "tp"),
        P("sp", "tp", None),
    )
    out_specs = P(("grp", "sp", "tp"), None)
    return jax.shard_map(
        per_device, mesh=mesh, in_specs=in_specs, out_specs=out_specs, check_vma=False
    )
```

profile of v0, /device:TPU:0, one launch (start us, length us, event | category | flops | bytes accessed | tf_op | source)
XLA Modules:
  0.0 503.5 jit_solution(3561112254705816321)
XLA Ops:
  6.6 2.0 copy.36
  8.6 1.8 copy.38
  10.5 1.8 copy.39
  12.4 1.8 copy.41
  17.5 24.9 %all-gather.6.cloned.1.call-done = bf16[2048,2,256]{0,2,1:T(8,128)(2,1)} async-done(((bf16[256,2,256]{0,2,1:T(8,128)(2,1)}), bf16[2048,2,256]{0,2,1:T(8,128)(2,1)}) %all-gather.6.cloned.1.call-update) | async-done | bytes 2097168 | tf_op jit(solution)/shard_map/all_gather | solution.py:149
  42.4 31.3 %all-gather.8.cloned.1.call-done = bf16[2048,512]{0,1:T(8,128)(2,1)} async-done(((bf16[256,512]{0,1:T(8,128)(2,1)}), bf16[2048,512]{0,1:T(8,128)(2,1)}) %all-gather.8.cloned.1.call-update) | async-done | bytes 2097168 | tf_op jit(solution)/shard_map/all_gather | solution.py:150
  73.7 31.3 %all-gather.10.cloned.1.call-done = bf16[2048,2,256]{0,2,1:T(8,128)(2,1)} async-done(((bf16[256,2,256]{0,2,1:T(8,128)(2,1)}), bf16[2048,2,256]{0,2,1:T(8,128)(2,1)}) %all-gather.10.cloned.1.call-update) | async-done | bytes 2097168 | tf_op jit(solution)/shard_map/all_gather | solution.py:151
  104.9 31.1 %all-gather.12.cloned.1.call-done = bf16[2048,512]{0,1:T(8,128)(2,1)} async-done(((bf16[256,512]{0,1:T(8,128)(2,1)}), bf16[2048,512]{0,1:T(8,128)(2,1)}) %all-gather.12.cloned.1.call-update) | async-done | bytes 2097168 | tf_op jit(solution)/shard_map/all_gather | solution.py:152
  137.3 13.8 %while.24 = (s32[]{:T(128)}, f32[2,256,2]{1,2,0:T(2,128)S(1)}, f32[2,256,2]{1,2,0:T(2,128)S(1)}, f32[2,256,2,256]{3,1,0,2:T(8,128)S(1)}, f32[2,256,4]{1,2,0:T(4,...) while((s32[]{:T(128)}, f32[2,256,2]{1,2,0:T(2,128)S(1)}, ...), condition=%wide.region_7.8_spmd.clone, body=%wide.region_0.7_spmd.clone.sunk | while | flops 1640242432 | bytes 83845752 | solution.py:173
  137.3 13.8 %conditional.3 = ((f32[2,256,2]{1,2,0:T(2,128)S(1)}, f32[2,256,2]{1,2,0:T(2,128)S(1)}, f32[2,256,2,256]{3,1,0,2:T(8,128)S(1)}, f32[2,256,4]{1,2,0:T(4,128)S(1)},...) conditional(s32[]{:T(128)} %convert_element_type.151, (f32[2,256,2]{1,2,0:T(2,128)S(1)}, ...), branch_computations={%region_1.0_spmd, %region_2.6_spmd} | conditional | flops 1640242432 | bytes 83844368 | solution.py:170
  137.5 1.8 constant_dynamic-slice_fusion.1
  142.7 1.3 fusion.15
  144.1 1.5 fusion.2
  145.6 2.3 fusion.3
  148.0 2.0 fusion.21
  152.4 2.3 fusion.84
  154.7 1.4 fusion.65
  156.0 1.6 copy.45
  157.9 1.5 fusion.57
  160.4 1.7 fusion.34
  162.6 1.3 reduce-window.16
  165.9 29.2 %reduce-scatter.3.cloned.1.call-done = bf16[128,2048]{1,0:T(8,128)(2,1)} async-done(((bf16[256,2048]{1,0:T(8,128)(2,1)}), bf16[128,2048]{1,0:T(8,128)(2,1)}) %reduce-scatter.3.cloned.1.call-update) | async-done | bytes 524304 | tf_op jit(solution)/shard_map/reduce_scatter | solution.py:176
  196.4 1.5 fusion.42
  197.8 3.0 convolution_convert_fusion.1
  200.8 65.0 %all_to_all.10 = bf16[8,80,2048]{2,1,0:T(8,128)(2,1)} all-to-all(bf16[8,80,2048]{2,1,0:T(8,128)(2,1)} %bitcast.199), channel_id=1, replica_groups=mesh['grp'=2,'sp'=8,'tp'=2] {'sp'}, dimensions={0} | all-to-all | bytes 5242880 | tf_op jit(solution)/shard_map/all_to_all | solution.py:196
  265.9 66.6 %all-gather.14.cloned.1.call-done = bf16[1280,2048]{1,0:T(8,128)(2,1)} async-done(((bf16[640,2048]{1,0:T(8,128)(2,1)}), bf16[1280,2048]{1,0:T(8,128)(2,1)}) %all-gather.14.cloned.1.call-update) | async-done | bytes 5242896 | tf_op jit(solution)/shard_map/all_gather | solution.py:198
  332.5 10.2 %fusion.26 = f32[1280,1024]{1,0:T(8,128)} fusion(bf16[1280,2048]{1,0:T(8,128)(2,1)} %all-gather.14.cloned.1.call-done, bf16[1,2048,1024]{2,1,0:T(8,128)(2,1)} %param.41), kind=kOutput, calls=%fused_computation.34 | convolution fusion | flops 5368709120 | bytes 14680064 | tf_op jit(solution)/shard_map/dot_general | solution.py:199
  342.7 18.7 %convolution_convert_fusion = bf16[1280,2048]{1,0:T(8,128)(2,1)} fusion(bf16[1,1024,2048]{2,1,0:T(8,128)(2,1)} %param.43, f32[1280,1024]{1,0:T(8,128)} %fusion.26, bf16[1280,2048]{1,0:T(8,128)(2,1)} %all-gather.14.cloned.1.call-done, bf16[1,2048,1024]{2,1,0:T(8,128)(2,1)} %param.42), kind=kOutput, calls=%fused_computation.30 | convolution fusion | flops 10753146880 | bytes 24117248 | tf_op jit(solution)/shard_map/dot_general | solution.py:204
  361.4 65.9 %reduce-scatter.5.cloned.1.call-done = bf16[640,2048]{1,0:T(8,128)(2,1)} async-done(((bf16[1280,2048]{1,0:T(8,128)(2,1)}), bf16[640,2048]{1,0:T(8,128)(2,1)}) %reduce-scatter.5.cloned.1.call-update) | async-done | bytes 2621456 | tf_op jit(solution)/shard_map/reduce_scatter | solution.py:205
  427.3 4.7 all-to-all-start.1
  433.1 59.3 %all-to-all-done.1 = bf16[8,80,2048]{2,1,0:T(8,128)(2,1)} async-done(((bf16[8,80,2048]{2,1,0:T(8,128)(2,1)}), bf16[8,80,2048]{2,1,0:T(8,128)(2,1)}, u32[]{:S(2)}, u32[]{:S(2)}) %all-to-all-start.1) | async-done | bytes 2621472 | tf_op jit(solution)/shard_map/all_to_all | solution.py:207
  492.4 3.2 multiply_reduce_fusion
  (117 shorter events, 17.5 us)
Async XLA Ops:
  6.5 152.9 %copy-start = (bf16[512,2048]{1,0:T(8,128)(2,1)S(1)}, bf16[512,2048]{1,0:T(8,128)(2,1)}, u32[]{:S(2)}) copy-start(bf16[512,2048]{1,0:T(8,128)(2,1)} %param.33) | copy-start | bytes 6291460
  6.5 9.7 %copy-start.9 = (bf16[256,2,256]{2,1,0:T(2,128)(2,1)S(1)}, bf16[256,2,256]{2,1,0:T(2,128)(2,1)}, u32[]{:S(2)}) copy-start(bf16[256,2,256]{2,1,0:T(2,128)(2,1)} %param.27) | copy-start | bytes 786436
  6.5 10.6 %copy-start.15 = (f32[256]{0:T(256)S(1)}, f32[256]{0:T(256)}, u32[]{:S(2)}) copy-start(f32[256]{0:T(256)} %param.31) | copy-start | bytes 3076
  6.5 10.6 %copy-start.17 = (f32[12]{0:T(128)S(1)}, f32[12]{0:T(128)}, u32[]{:S(2)}) copy-start(f32[12]{0:T(128)} %param.30) | copy-start | bytes 148
  6.5 10.8 %copy-start.16 = (f32[128]{0:T(128)S(1)}, f32[128]{0:T(128)}, u32[]{:S(2)}) copy-start(f32[128]{0:T(128)} %param.32) | copy-start | bytes 1540
  6.5 35.8 %all-gather.6.cloned.1.call-start = ((), (), s32[]{:S(2)}) async-start(), calls=%async_computation.4 | async-start | bytes 2359296 | tf_op jit(solution)/shard_map/all_gather | solution.py:149
  8.6 65.1 %all-gather.8.cloned.1.call-start = ((), (), s32[]{:S(2)}) async-start(), calls=%async_computation.5 | async-start | bytes 2359296 | tf_op jit(solution)/shard_map/all_gather | solution.py:150
  10.5 94.5 %all-gather.10.cloned.1.call-start = ((), (), s32[]{:S(2)}) async-start(), calls=%async_computation.6 | async-start | bytes 2359296 | tf_op jit(solution)/shard_map/all_gather | solution.py:151
  12.4 123.7 %all-gather.12.cloned.1.call-start = ((), (), s32[]{:S(2)}) async-start(), calls=%async_computation.7 | async-start | bytes 2359296 | tf_op jit(solution)/shard_map/all_gather | solution.py:152
  14.3 180.8 %reduce-scatter.3.cloned.1.call-start = ((), (), s32[]{:S(2)}) async-start(), calls=%async_computation.8 | async-start | bytes 1572864 | tf_op jit(solution)/shard_map/reduce_scatter | solution.py:176
  137.5 1.8 copy-start.3
  140.3 1.6 copy-start.1
  140.3 2.2 copy-start.2
  142.5 1.6 copy-start.4
  145.6 2.4 copy-start.5
  150.0 1.0 copy-start.6
  157.7 2.7 copy-start.7
  160.2 2.0 copy-start.13
  160.2 36.2 %copy-start.8 = (bf16[128,2048]{1,0:T(8,128)(2,1)S(1)}, bf16[128,2048]{1,0:T(8,128)(2,1)}, u32[]{:S(2)}) copy-start(bf16[128,2048]{1,0:T(8,128)(2,1)} %param.35) | copy-start | bytes 1572868
  160.2 36.2 %copy-start.10 = (f32[2048]{0:T(1024)S(1)}, f32[2048]{0:T(1024)}, u32[]{:S(2)}) copy-start(f32[2048]{0:T(1024)} %param.36) | copy-start | bytes 24580
  160.4 37.4 %copy-start.11 = (f32[2048]{0:T(1024)S(1)}, f32[2048]{0:T(1024)}, u32[]{:S(2)}) copy-start(f32[2048]{0:T(1024)} %param.37) | copy-start | bytes 24580
  162.2 170.3 %all-gather.14.cloned.1.call-start = ((), (), s32[]{:S(2)}) async-start(), calls=%async_computation.9 | async-start | bytes 7864320 | tf_op jit(solution)/shard_map/all_gather | solution.py:198
  265.8 161.5 %reduce-scatter.5.cloned.1.call-start = ((), (), s32[]{:S(2)}) async-start(), calls=%async_computation.10 | async-start | bytes 7864320 | tf_op jit(solution)/shard_map/reduce_scatter | solution.py:205
  361.4 70.7 %copy-start.14 = (f32[128,4]{0,1:T(4,128)S(1)}, f32[128,4]{0,1:T(4,128)}, u32[]{:S(2)}) copy-start(f32[128,4]{0,1:T(4,128)} %param.40) | copy-start | bytes 6148
  427.3 68.3 %copy-start.12 = (f32[2048]{0:T(1024)S(1)}, f32[2048]{0:T(1024)}, u32[]{:S(2)}) copy-start(f32[2048]{0:T(1024)} %param.38) | copy-start | bytes 24580
  427.3 65.1 %all-to-all-start.1 = ((bf16[8,80,2048]{2,1,0:T(8,128)(2,1)}), bf16[8,80,2048]{2,1,0:T(8,128)(2,1)}, u32[]{:S(2)}, u32[]{:S(2)}) async-start(bf16[8,80,2048]{2,1,0:T(8,128)(2,1)} %bitcast.202), calls=%async_computation.3 | async-start | bytes 5242880 | tf_op jit(solution)/shard_map/all_to_all | solution.py:207
Sparse Core Ops, SparseCore 0:
  8.9 33.3 all-gather.5
  44.0 29.6 all-gather.7
  75.3 29.6 all-gather.9
  106.4 29.6 all-gather.11
  162.3 32.7 reduce-scatter.2
  266.0 66.4 all-gather.13
  361.5 65.7 reduce-scatter.4
where the time goes:
time: 504 us
  waiting for transfers between devices  340 us (67%)
  blocking collectives  65 us (13%)
  matrix products  44.2 us (9%)
  local copies, waits for them, and re-layouts  22.1 us (4%)
  between operations  13.8 us (3%)
  other arithmetic  13.5 us (3%)
  starting transfers between devices  5.04 us (1%)
    all_gather x1, waiting for transfers between devices, per_device(): lax.all_gather(arrived.reshape(-1, columns), 'tp', axis=0, tiled=True)  66.6 us
    reduce_scatter x1, waiting for transfers between devices, per_device(): lax.psum_scatter(partials.astype(jnp.bfloat16), 'tp', scatter_dimension=0...  65.9 us
    all_to_all x1, blocking collectives, per_device(): lax.all_to_all(outgoing, 'sp', split_axis=0, concat_axis=0, tiled=True)  65 us
    all_to_all x1, waiting for transfers between devices, per_device(): lax.all_to_all(results, 'sp', split_axis=0, concat_axis=0, tiled=True)  59.3 us
    all_gather x1, waiting for transfers between devices, per_device(): lax.all_gather(values_a, 'sp', axis=0, tiled=True)  31.3 us
    all_gather x1, waiting for transfers between devices, per_device(): lax.all_gather(keys_b, 'sp', axis=0, tiled=True)  31.3 us
    all_gather x1, waiting for transfers between devices, per_device(): lax.all_gather(values_b, 'sp', axis=0, tiled=True)  31.1 us
    reduce_scatter x1, waiting for transfers between devices, per_device(): lax.psum_scatter((jnp.dot(heads_out_a, out_a, preferred_element_type=jnp....  29.2 us
  transfers between devices with their start and end apart: 8, of which 8 were waited for; matrix products, arithmetic and copies ran while one was open for 3% of the time, Pallas kernels for 0%

commit v1 on v0

--- a/solution.py
+++ b/solution.py
@@ -6,6 +6,19 @@
 HA = 4
 DA = 128
 DB = 64
+
+
+def ring_gather(shard, axis, dim):
+    count, index, rows = (lax.axis_size(axis), lax.axis_index(axis), shard.shape[dim])
+    right = [(i, (i + 1) % count) for i in range(count)]
+    out = jnp.zeros((*shard.shape[:dim], count * rows, *shard.shape[dim + 1 :]), shard.dtype)
+    block = shard
+    for lap in range(count):
+        source = (index - lap) % count
+        out = lax.dynamic_update_slice_in_dim(out, block, source * rows, axis=dim)
+        if lap < count - 1:
+            block = lax.ppermute(block, axis, right)
+    return out
 
 
 def rms_norm(values, gain_vec):
@@ -148,7 +161,7 @@
     pieces = (
         lax.all_gather(keys_a, "sp", axis=0, tiled=True),
         lax.all_gather(values_a, "sp", axis=0, tiled=True),
-        lax.all_gather(keys_b, "sp", axis=0, tiled=True),
+        ring_gather(keys_b, "sp", 0),
         lax.all_gather(values_b, "sp", axis=0, tiled=True),
     )
     key_count = pieces[0].shape[0]

time: 504 us -> 483 us (0.958)
  waiting for transfers between devices: 340 us -> 307 us
  local copies, waits for them, and re-layouts: 22.1 us -> 32.2 us
    ppermute x0 -> x7, waiting for transfers between devices: none -> 60 us  [ring_gather(): block = lax.ppermute(block, axis, right)]
    all_gather x1, waiting for transfers between devices: 31.3 us -> 0.01 us  [per_device(): lax.all_gather(values_a, 'sp', axis=0, tiled=True)]
    all_gather x1 -> x0, waiting for transfers between devices: 31.3 us -> none  [per_device(): lax.all_gather(keys_b, 'sp', axis=0, tiled=True)]
    all_gather x1, waiting for transfers between devices: 24.9 us -> 0.01 us  [per_device(): lax.all_gather(keys_a, 'sp', axis=0, tiled=True)]
    dynamic_update_slice x0 -> x8, local copies, waits for them, and re-layouts: none -> 6.96 us  [ring_gather(): out = lax.dynamic_update_slice_in_dim(out, block, source * rows, axis=dim)]
    unnamed x37 -> x33, local copies, waits for them, and re-layouts: 10.6 us -> 11.4 us
  transfers between devices with their start and end apart: 8 -> 14, of which waited for: 8 -> 12; matrix products, arithmetic and copies ran while one was open for 3% -> 5% of each run, Pallas kernels for 0% -> 0%
where the time goes in v1:
time: 483 us; the launch traced here: 482 us
  waiting for transfers between devices  307 us (64%)
  blocking collectives  65 us (13%)
  matrix products  44.2 us (9%)
  local copies, waits for them, and re-layouts  32.2 us (7%)
  between operations  13.7 us (3%)
  other arithmetic  13.4 us (3%)
  starting transfers between devices  5.78 us (1%)
    all_gather x1, waiting for transfers between devices, per_device(): lax.all_gather(arrived.reshape(-1, columns), 'tp', axis=0, tiled=True)  66.6 us
    reduce_scatter x1, waiting for transfers between devices, per_device(): lax.psum_scatter(partials.astype(jnp.bfloat16), 'tp', scatter_dimension=0...  65.9 us
    all_to_all x1, blocking collectives, per_device(): lax.all_to_all(outgoing, 'sp', split_axis=0, concat_axis=0, tiled=True)  65 us
    ppermute x7, waiting for transfers between devices, ring_gather(): block = lax.ppermute(block, axis, right)  60 us
    all_to_all x1, waiting for transfers between devices, per_device(): lax.all_to_all(results, 'sp', split_axis=0, concat_axis=0, tiled=True)  59.3 us
    reduce_scatter x1, waiting for transfers between devices, per_device(): lax.psum_scatter((jnp.dot(heads_out_a, out_a, preferred_element_type=jnp....  29.2 us
    all_gather x1, waiting for transfers between devices, per_device(): lax.all_gather(values_b, 'sp', axis=0, tiled=True)  26.2 us
    dot_general x1, matrix products, per_device(): jnp.dot(hidden, expert_down[0], preferred_element_type=jnp.float32)  18.7 us
  transfers between devices with their start and end apart: 14, of which 12 were waited for; matrix products, arithmetic and copies ran while one was open for 5% of the time, Pallas kernels for 0%

profile of v1, /device:TPU:0, one launch (start us, length us, event | category | flops | bytes accessed | tf_op | source)
XLA Modules:
  0.0 481.8 jit_solution(8793037957856792346)
XLA Ops:
  6.5 2.0 copy.37
  8.6 1.8 copy.39
  10.5 1.8 copy.43
  14.0 8.1 %collective-permute-done = bf16[256,2,256]{0,2,1:T(8,128)(2,1)S(1)} collective-permute-done((bf16[256,2,256]{0,2,1:T(8,128)(2,1)S(1)}, bf16[256,2,256]{0,2,1:T(8,128)(2,1)S(1)}, u32[]{:S(2)}, u32[]{:S(2)}) %collective-permute-start) | collective-permute-done | bytes 262176 | tf_op jit(solution)/shard_map/ppermute | solution.py:20
  22.1 12.9 %collective-permute-done.1 = bf16[256,2,256]{0,2,1:T(8,128)(2,1)S(1)} collective-permute-done((bf16[256,2,256]{0,2,1:T(8,128)(2,1)S(1)}, bf16[256,2,256]{0,2,1:T(8,128)(2,1)S(1)}, u32[]{:S(2)}, u32[]{:S(2)}) %collective-permute-start.1) | collective-permute-done | bytes 262176 | tf_op jit(solution)/shard_map/ppermute | solution.py:20
  35.8 10.4 %collective-permute-done.2 = bf16[256,2,256]{0,2,1:T(8,128)(2,1)S(1)} collective-permute-done((bf16[256,2,256]{0,2,1:T(8,128)(2,1)S(1)}, bf16[256,2,256]{0,2,1:T(8,128)(2,1)S(1)}, u32[]{:S(2)}, u32[]{:S(2)}) %collective-permute-start.2) | collective-permute-done | bytes 262176 | tf_op jit(solution)/shard_map/ppermute | solution.py:20
  47.0 6.8 %collective-permute-done.3 = bf16[256,2,256]{0,2,1:T(8,128)(2,1)S(1)} collective-permute-done((bf16[256,2,256]{0,2,1:T(8,128)(2,1)S(1)}, bf16[256,2,256]{0,2,1:T(8,128)(2,1)S(1)}, u32[]{:S(2)}, u32[]{:S(2)}) %collective-permute-start.3) | collective-permute-done | bytes 262176 | tf_op jit(solution)/shard_map/ppermute | solution.py:20
  53.8 1.6 broadcast_in_dim.120
  58.1 1.8 copy.42
  60.1 6.0 %collective-permute-done.4 = bf16[256,2,256]{0,2,1:T(8,128)(2,1)} collective-permute-done((bf16[256,2,256]{0,2,1:T(8,128)(2,1)S(1)}, bf16[256,2,256]{0,2,1:T(8,128)(2,1)}, u32[]{:S(2)}, u32[]{:S(2)}) %collective-permute-start.4) | collective-permute-done | bytes 262176 | tf_op jit(solution)/shard_map/ppermute | solution.py:20
  68.3 11.3 %collective-permute-done.5 = bf16[256,2,256]{0,2,1:T(8,128)(2,1)S(1)} collective-permute-done((bf16[256,2,256]{0,2,1:T(8,128)(2,1)}, bf16[256,2,256]{0,2,1:T(8,128)(2,1)S(1)}, u32[]{:S(2)}, u32[]{:S(2)}) %collective-permute-start.5) | collective-permute-done | bytes 262176 | tf_op jit(solution)/shard_map/ppermute | solution.py:20
  80.4 1.7 constant_dynamic-update-slice_fusion.2
  82.8 4.4 collective-permute-done.6
  88.0 26.2 %all-gather.9.cloned.1.call-done = bf16[2048,512]{0,1:T(8,128)(2,1)} async-done(((bf16[256,512]{0,1:T(8,128)(2,1)}), bf16[2048,512]{0,1:T(8,128)(2,1)}) %all-gather.9.cloned.1.call-update) | async-done | bytes 2097168 | tf_op jit(solution)/shard_map/all_gather | solution.py:165
  115.5 13.8 %while.24 = (s32[]{:T(128)}, f32[2,256,2]{1,2,0:T(2,128)S(1)}, f32[2,256,2]{1,2,0:T(2,128)S(1)}, f32[2,256,2,256]{3,1,0,2:T(8,128)S(1)}, f32[2,256,4]{1,2,0:T(4,...) while((s32[]{:T(128)}, f32[2,256,2]{1,2,0:T(2,128)S(1)}, ...), condition=%wide.region_7.8_spmd.clone, body=%wide.region_0.7_spmd.clone.sunk | while | flops 1640242432 | bytes 83845752 | solution.py:186
  115.5 13.8 %conditional.3 = ((f32[2,256,2]{1,2,0:T(2,128)S(1)}, f32[2,256,2]{1,2,0:T(2,128)S(1)}, f32[2,256,2,256]{3,1,0,2:T(8,128)S(1)}, f32[2,256,4]{1,2,0:T(4,128)S(1)},...) conditional(s32[]{:T(128)} %convert_element_type.151, (f32[2,256,2]{1,2,0:T(2,128)S(1)}, ...), branch_computations={%region_1.1_spmd, %region_2.6_spmd} | conditional | flops 1640242432 | bytes 83844368 | solution.py:183
  115.7 1.8 constant_dynamic-slice_fusion.1
  123.8 2.3 fusion.3
  126.2 2.0 fusion.21
  130.6 2.3 fusion.84
  134.2 1.6 copy.47
  138.6 1.7 fusion.34
  144.1 29.2 %reduce-scatter.3.cloned.1.call-done = bf16[128,2048]{1,0:T(8,128)(2,1)} async-done(((bf16[256,2048]{1,0:T(8,128)(2,1)}), bf16[128,2048]{1,0:T(8,128)(2,1)}) %reduce-scatter.3.cloned.1.call-update) | async-done | bytes 524304 | tf_op jit(solution)/shard_map/reduce_scatter | solution.py:189
  176.0 3.0 convolution_convert_fusion.1
  179.0 65.0 %all_to_all.10 = bf16[8,80,2048]{2,1,0:T(8,128)(2,1)} all-to-all(bf16[8,80,2048]{2,1,0:T(8,128)(2,1)} %bitcast.199), channel_id=1, replica_groups=mesh['grp'=2,'sp'=8,'tp'=2] {'sp'}, dimensions={0} | all-to-all | bytes 5242880 | tf_op jit(solution)/shard_map/all_to_all | solution.py:209
  244.1 66.6 %all-gather.11.cloned.1.call-done = bf16[1280,2048]{1,0:T(8,128)(2,1)} async-done(((bf16[640,2048]{1,0:T(8,128)(2,1)}), bf16[1280,2048]{1,0:T(8,128)(2,1)}) %all-gather.11.cloned.1.call-update) | async-done | bytes 5242896 | tf_op jit(solution)/shard_map/all_gather | solution.py:211
  310.7 10.2 %fusion.26 = f32[1280,1024]{1,0:T(8,128)} fusion(bf16[1280,2048]{1,0:T(8,128)(2,1)} %all-gather.11.cloned.1.call-done, bf16[1,2048,1024]{2,1,0:T(8,128)(2,1)} %param.41), kind=kOutput, calls=%fused_computation.34 | convolution fusion | flops 5368709120 | bytes 14680064 | tf_op jit(solution)/shard_map/dot_general | solution.py:212
  320.9 18.7 %convolution_convert_fusion = bf16[1280,2048]{1,0:T(8,128)(2,1)} fusion(bf16[1,1024,2048]{2,1,0:T(8,128)(2,1)} %param.43, f32[1280,1024]{1,0:T(8,128)} %fusion.26, bf16[1280,2048]{1,0:T(8,128)(2,1)} %all-gather.11.cloned.1.call-done, bf16[1,2048,1024]{2,1,0:T(8,128)(2,1)} %param.42), kind=kOutput, calls=%fused_computation.30 | convolution fusion | flops 10753146880 | bytes 24117248 | tf_op jit(solution)/shard_map/dot_general | solution.py:217
  339.6 65.9 %reduce-scatter.5.cloned.1.call-done = bf16[640,2048]{1,0:T(8,128)(2,1)} async-done(((bf16[1280,2048]{1,0:T(8,128)(2,1)}), bf16[640,2048]{1,0:T(8,128)(2,1)}) %reduce-scatter.5.cloned.1.call-update) | async-done | bytes 2621456 | tf_op jit(solution)/shard_map/reduce_scatter | solution.py:218
  405.6 4.8 all-to-all-start.1
  411.4 59.3 %all-to-all-done.1 = bf16[8,80,2048]{2,1,0:T(8,128)(2,1)} async-done(((bf16[8,80,2048]{2,1,0:T(8,128)(2,1)}), bf16[8,80,2048]{2,1,0:T(8,128)(2,1)}, u32[]{:S(2)}, u32[]{:S(2)}) %all-to-all-start.1) | async-done | bytes 2621472 | tf_op jit(solution)/shard_map/all_to_all | solution.py:220
  470.7 3.2 multiply_reduce_fusion
  (133 shorter events, 33.4 us)
Async XLA Ops:
  6.5 131.1 %copy-start = (bf16[512,2048]{1,0:T(8,128)(2,1)S(1)}, bf16[512,2048]{1,0:T(8,128)(2,1)}, u32[]{:S(2)}) copy-start(bf16[512,2048]{1,0:T(8,128)(2,1)} %param.33) | copy-start | bytes 6291460
  6.5 53.4 %copy-start.15 = (f32[12]{0:T(128)S(1)}, f32[12]{0:T(128)}, u32[]{:S(2)}) copy-start(f32[12]{0:T(128)} %param.30) | copy-start | bytes 148
  6.5 53.5 %copy-start.14 = (f32[128]{0:T(128)S(1)}, f32[128]{0:T(128)}, u32[]{:S(2)}) copy-start(f32[128]{0:T(128)} %param.32) | copy-start | bytes 1540
  6.5 81.4 %all-gather.5.cloned.1.call-start = ((), (), s32[]{:S(2)}) async-start(), calls=%async_computation.4 | async-start | bytes 2359296 | tf_op jit(solution)/shard_map/all_gather | solution.py:162
  8.5 79.4 %all-gather.7.cloned.1.call-start = ((), (), s32[]{:S(2)}) async-start(), calls=%async_computation.5 | async-start | bytes 2359296 | tf_op jit(solution)/shard_map/all_gather | solution.py:163
  10.4 103.8 %all-gather.9.cloned.1.call-start = ((), (), s32[]{:S(2)}) async-start(), calls=%async_computation.6 | async-start | bytes 2359296 | tf_op jit(solution)/shard_map/all_gather | solution.py:165
  12.3 161.0 %reduce-scatter.3.cloned.1.call-start = ((), (), s32[]{:S(2)}) async-start(), calls=%async_computation.7 | async-start | bytes 1572864 | tf_op jit(solution)/shard_map/reduce_scatter | solution.py:189
  13.5 8.6 %collective-permute-start = (bf16[256,2,256]{0,2,1:T(8,128)(2,1)S(1)}, bf16[256,2,256]{0,2,1:T(8,128)(2,1)S(1)}, u32[]{:S(2)}, u32[]{:S(2)}) collective-permute-start(bf16[256,2,256]{0,2,1:T(8,128)(2,1)S(1)} %copy.40), channel_id=1, source_target_pairs={{0,2},{2,4},{4,6},{6,8},{8,10},{10,12},{12,14},{14,0},{1,3},{3,5},... | collective-permute-start | bytes 786440 | tf_op jit(solution)/shard_map/ppermute | solution.py:20
  22.1 12.9 %collective-permute-start.1 = (bf16[256,2,256]{0,2,1:T(8,128)(2,1)S(1)}, bf16[256,2,256]{0,2,1:T(8,128)(2,1)S(1)}, u32[]{:S(2)}, u32[]{:S(2)}) collective-permute-start(bf16[256,2,256]{0,2,1:T(8,128)(2,1)S(1)} %collective-permute-done), channel_id=1, source_target_pairs={{0,2},{2,4},{4,6},{6,8},{8,10},{10,12},{12,14},{14,0},{1,3},{3,5},... | collective-permute-start | bytes 786440 | tf_op jit(solution)/shard_map/ppermute | solution.py:20
  35.1 11.2 %collective-permute-start.2 = (bf16[256,2,256]{0,2,1:T(8,128)(2,1)S(1)}, bf16[256,2,256]{0,2,1:T(8,128)(2,1)S(1)}, u32[]{:S(2)}, u32[]{:S(2)}) collective-permute-start(bf16[256,2,256]{0,2,1:T(8,128)(2,1)S(1)} %collective-permute-done.1), channel_id=1, source_target_pairs={{0,2},{2,4},{4,6},{6,8},{8,10},{10,12},{12,14},{14,0},{1,3},{3,5},... | collective-permute-start | bytes 786440 | tf_op jit(solution)/shard_map/ppermute | solution.py:20
  46.2 7.6 %collective-permute-start.3 = (bf16[256,2,256]{0,2,1:T(8,128)(2,1)S(1)}, bf16[256,2,256]{0,2,1:T(8,128)(2,1)S(1)}, u32[]{:S(2)}, u32[]{:S(2)}) collective-permute-start(bf16[256,2,256]{0,2,1:T(8,128)(2,1)S(1)} %collective-permute-done.2), channel_id=1, source_target_pairs={{0,2},{2,4},{4,6},{6,8},{8,10},{10,12},{12,14},{14,0},{1,3},{3,5},... | collective-permute-start | bytes 786440 | tf_op jit(solution)/shard_map/ppermute | solution.py:20
  53.8 12.3 %collective-permute-start.4 = (bf16[256,2,256]{0,2,1:T(8,128)(2,1)S(1)}, bf16[256,2,256]{0,2,1:T(8,128)(2,1)}, u32[]{:S(2)}, u32[]{:S(2)}) collective-permute-start(bf16[256,2,256]{0,2,1:T(8,128)(2,1)S(1)} %collective-permute-done.3), channel_id=1, source_target_pairs={{0,2},{2,4},{4,6},{6,8},{8,10},{10,12},{12,14},{14,0},{1,3},{3,5},... | collective-permute-start | bytes 786440 | tf_op jit(solution)/shard_map/ppermute | solution.py:20
  66.1 13.6 %collective-permute-start.5 = (bf16[256,2,256]{0,2,1:T(8,128)(2,1)}, bf16[256,2,256]{0,2,1:T(8,128)(2,1)S(1)}, u32[]{:S(2)}, u32[]{:S(2)}) collective-permute-start(bf16[256,2,256]{0,2,1:T(8,128)(2,1)} %collective-permute-done.4), channel_id=1, source_target_pairs={{0,2},{2,4},{4,6},{6,8},{8,10},{10,12},{12,14},{14,0},{1,3},{3,5},... | collective-permute-start | bytes 786440 | tf_op jit(solution)/shard_map/ppermute | solution.py:20
  79.6 7.6 %collective-permute-start.6 = (bf16[256,2,256]{0,2,1:T(8,128)(2,1)S(1)}, bf16[256,2,256]{0,2,1:T(8,128)(2,1)S(1)}, u32[]{:S(2)}, u32[]{:S(2)}) collective-permute-start(bf16[256,2,256]{0,2,1:T(8,128)(2,1)S(1)} %collective-permute-done.5), channel_id=1, source_target_pairs={{0,2},{2,4},{4,6},{6,8},{8,10},{10,12},{12,14},{14,0},{1,3},{3,5},... | collective-permute-start | bytes 786440 | tf_op jit(solution)/shard_map/ppermute | solution.py:20
  115.7 1.8 copy-start.3
  118.4 1.6 copy-start.1
  118.5 2.2 copy-start.2
  120.7 1.6 copy-start.4
  123.8 2.4 copy-start.5
  128.2 1.1 copy-start.6
  135.9 2.7 copy-start.7
  138.3 2.3 copy-start.12
  138.4 36.2 %copy-start.8 = (bf16[128,2048]{1,0:T(8,128)(2,1)S(1)}, bf16[128,2048]{1,0:T(8,128)(2,1)}, u32[]{:S(2)}) copy-start(bf16[128,2048]{1,0:T(8,128)(2,1)} %param.35) | copy-start | bytes 1572868
  138.4 36.2 %copy-start.9 = (f32[2048]{0:T(1024)S(1)}, f32[2048]{0:T(1024)}, u32[]{:S(2)}) copy-start(f32[2048]{0:T(1024)} %param.36) | copy-start | bytes 24580
  138.6 37.4 %copy-start.10 = (f32[2048]{0:T(1024)S(1)}, f32[2048]{0:T(1024)}, u32[]{:S(2)}) copy-start(f32[2048]{0:T(1024)} %param.37) | copy-start | bytes 24580
  140.3 170.4 %all-gather.11.cloned.1.call-start = ((), (), s32[]{:S(2)}) async-start(), calls=%async_computation.8 | async-start | bytes 7864320 | tf_op jit(solution)/shard_map/all_gather | solution.py:211
  244.0 161.5 %reduce-scatter.5.cloned.1.call-start = ((), (), s32[]{:S(2)}) async-start(), calls=%async_computation.9 | async-start | bytes 7864320 | tf_op jit(solution)/shard_map/reduce_scatter | solution.py:218
  339.6 70.8 %copy-start.13 = (f32[128,4]{0,1:T(4,128)S(1)}, f32[128,4]{0,1:T(4,128)}, u32[]{:S(2)}) copy-start(f32[128,4]{0,1:T(4,128)} %param.40) | copy-start | bytes 6148
  405.6 68.4 %copy-start.11 = (f32[2048]{0:T(1024)S(1)}, f32[2048]{0:T(1024)}, u32[]{:S(2)}) copy-start(f32[2048]{0:T(1024)} %param.38) | copy-start | bytes 24580
  405.6 65.1 %all-to-all-start.1 = ((bf16[8,80,2048]{2,1,0:T(8,128)(2,1)}), bf16[8,80,2048]{2,1,0:T(8,128)(2,1)}, u32[]{:S(2)}, u32[]{:S(2)}) async-start(bf16[8,80,2048]{2,1,0:T(8,128)(2,1)} %bitcast.202), calls=%async_computation.3 | async-start | bytes 5242880 | tf_op jit(solution)/shard_map/all_to_all | solution.py:220
Sparse Core Ops, SparseCore 0:
  8.9 38.1 all-gather.4
  48.7 33.9 all-gather.6
  84.3 29.8 all-gather.8
  140.5 32.7 reduce-scatter.2
  244.2 66.5 all-gather.10
  339.8 65.7 reduce-scatter.4
